TPU v7x, 32 devices: a whole 2x2x4 slice. The times are simulated.
32 devices in a mesh: sp: 8 (over z, core), tp: 4 (over y, x).
Axes of the slice: x: 2, y: 2, z: 4, core: 2. Of those that a mesh axis runs over, the one named last changes fastest.
Arguments:
- tokens: bfloat16 [2048, 1024], P('sp', 'tp'), may hold values from -6 to 6
- norm_gain: bfloat16 [2, 1024], P(None, 'tp'), may hold values from 0.099609375 to 1.8984375
- query_weight: bfloat16 [2, 1024, 1024], P(None, 'sp', 'tp'), may hold values from -0.1875 to 0.1875
- key_weight: bfloat16 [2, 1024, 1024], P(None, 'sp', 'tp'), may hold values from -0.1875 to 0.1875
- value_weight: bfloat16 [2, 1024, 1024], P(None, 'sp', 'tp'), may hold values from -0.1875 to 0.1875
- output_weight: bfloat16 [2, 1024, 1024], P(None, 'tp', 'sp'), may hold values from -0.5 to 0.5
- offset_bias: float32 [2, 16, 15, 31], P(None, 'tp'), may hold values from -4 to 4
Outputs:
- mixed: bfloat16 [2048, 1024], P('sp', 'tp')
All inputs are finite; a program needn't handle non-finite values.
Results may differ from a plain program's by a relative error of at most 0.03.
Values may be sent and summed in bfloat16 or wider, within the bound.
A program may use at most 64 MiB of HBM per device.

v0:
```python
import jax
import jax.numpy as jnp
from jax import lax
from jax.sharding import PartitionSpec as P

HEAD_DIM = 64
WIN_H = 8
WIN_W = 16
ROWS_DEV = 4
COLS = 64
D = 1024


norm_eps = 1e-06


def folded(value, axis, dim, update, carry):
    whole = jax.tree.map(lambda part: lax.all_gather(part, axis, axis=dim, tiled=True), value)
    return update(carry, whole, jnp.int32(0))


def extended(block, sides, width, periodic):
    for axis, dim in sides:
        count = lax.axis_size(axis)
        forward = [(i, i + 1) for i in range(count - 1)]
        if periodic:
            forward.append((count - 1, 0))
        backward = [(target, source) for source, target in forward]
        low = lax.ppermute(
            lax.slice_in_dim(block, block.shape[dim] - width, None, axis=dim), axis, forward
        )
        high = lax.ppermute(lax.slice_in_dim(block, 0, width, axis=dim), axis, backward)
        block = jnp.concatenate([low, block, high], axis=dim)
    return block


def own_rows(portion, rows, axis):
    count = rows * lax.axis_size(axis)
    sent = portion(jnp.int32(0), count).astype(jnp.bfloat16)
    return lax.psum_scatter(sent, axis, scatter_dimension=0, tiled=True).astype(jnp.float32)


def attend(query, padded, table, base, total_rows):
    heads = table.shape[0]
    local_width = heads * HEAD_DIM
    half = WIN_H // 2
    span_rows = ROWS_DEV + WIN_H
    glob = base + jnp.arange(ROWS_DEV, dtype=jnp.int32)
    first = jnp.clip(glob - half, 0, total_rows - WIN_H).astype(jnp.int32)
    local_first = first - base + half
    padded_row = jnp.arange(span_rows, dtype=jnp.int32)
    row_inside = (padded_row[None, :] >= local_first[:, None]) & (
        padded_row[None, :] < local_first[:, None] + WIN_H
    )
    row_offset = padded_row[None, :] + base - half - glob[:, None] + (WIN_H - 1)
    row_codes = jnp.arange(2 * WIN_H - 1, dtype=jnp.int32)
    row_onehot = (row_offset[:, :, None] == row_codes[None, None, :]).astype(jnp.float32)
    column = jnp.arange(COLS, dtype=jnp.int32)
    col_start = jnp.clip(column - WIN_W // 2, 0, COLS - WIN_W).astype(jnp.int32)
    col_inside = (column[None, :] >= col_start[:, None]) & (
        column[None, :] < col_start[:, None] + WIN_W
    )
    col_offset = column[None, :] - column[:, None] + (WIN_W - 1)
    col_codes = jnp.arange(2 * WIN_W - 1, dtype=jnp.int32)
    col_onehot = (col_offset[:, :, None] == col_codes[None, None, :]).astype(jnp.float32)
    bias = jnp.einsum(
        "hab,ria,qkb->rhqik", table, row_onehot, col_onehot, precision=lax.Precision.HIGHEST
    )
    inside = row_inside[:, None, None, :, None] & col_inside[None, None, :, None, :]
    keys = padded[:, :, :local_width].reshape(span_rows, COLS, heads, HEAD_DIM)
    values = padded[:, :, local_width:].reshape(span_rows, COLS, heads, HEAD_DIM)
    grid_query = query.reshape(ROWS_DEV, COLS, heads, HEAD_DIM)
    score = jnp.einsum(
        "rqhd,ikhd->rhqik", grid_query, keys, preferred_element_type=jnp.float32
    ) * HEAD_DIM ** (-0.5)
    score = jnp.where(inside, score + bias, -1e30)
    flat = score.reshape(ROWS_DEV, heads, COLS, span_rows * COLS)
    weights = jax.nn.softmax(flat, axis=-1).reshape(score.shape).astype(jnp.bfloat16)
    out = jnp.einsum(
        "rhqik,ikhd->rqhd", weights, values, preferred_element_type=jnp.float32
    ).astype(jnp.bfloat16)
    return out.reshape(ROWS_DEV * COLS, local_width)


def body(tokens, norm_gain, query_weight, key_weight, value_weight, output_weight, offset_bias):
    layers = query_weight.shape[0]
    local_width = query_weight.shape[2]
    feature_rows = tokens.shape[1]
    token_count = tokens.shape[0]
    half = WIN_H // 2
    base = lax.axis_index("sp") * ROWS_DEV
    total_rows = ROWS_DEV * lax.axis_size("sp")
    every = (
        lax.all_gather(query_weight, "sp", axis=1, tiled=True),
        lax.all_gather(key_weight, "sp", axis=1, tiled=True),
        lax.all_gather(value_weight, "sp", axis=1, tiled=True),
        lax.all_gather(output_weight, "sp", axis=2, tiled=True),
    )
    current = tokens
    for layer in range(layers):
        query_full = every[0][layer]
        key_full = every[1][layer]
        value_full = every[2][layer]
        output_full = every[3][layer]
        stacked = jnp.concatenate([query_full, key_full, value_full], axis=1)
        floats = current.astype(jnp.float32)
        squares = lax.psum(jnp.sum(floats * floats, axis=1), "tp")
        factor = lax.rsqrt(squares / D + norm_eps)
        normed = (floats * factor[:, None] * norm_gain[layer].astype(jnp.float32)).astype(
            jnp.bfloat16
        )
        table = offset_bias[layer].astype(jnp.float32)

        def project(carry, piece, start):
            weight_rows = lax.dynamic_slice_in_dim(stacked, start, piece.shape[1], 0)
            return carry + jnp.dot(piece, weight_rows, preferred_element_type=jnp.float32)

        projected = folded(
            normed, "tp", 1, project, jnp.zeros((token_count, 3 * local_width), jnp.float32)
        ).astype(jnp.bfloat16)
        query = projected[:, :local_width]
        pair = projected[:, local_width:].reshape(ROWS_DEV, COLS, 2 * local_width)
        padded = extended(pair, (("sp", 0),), half, False)
        attended = attend(query, padded, table, base, total_rows)

        def project_out(start, count):
            weight_cols = lax.dynamic_slice_in_dim(output_full, start, count, 1)
            return lax.dot_general(
                weight_cols, attended, (((0,), (1,)), ((), ())), preferred_element_type=jnp.float32
            )

        summed = own_rows(project_out, feature_rows, "tp")
        current = summed.T.astype(jnp.bfloat16)
    return current


def solution(mesh):
    in_specs = (
        P("sp", "tp"),
        P(None, "tp"),
        P(None, "sp", "tp"),
        P(None, "sp", "tp"),
        P(None, "sp", "tp"),
        P(None, "tp", "sp"),
        P(None, "tp", None, None),
    )
    out_specs = P("sp", "tp")
    return jax.shard_map(body, mesh=mesh, in_specs=in_specs, out_specs=out_specs, check_vma=False)
```

profile of v0, /device:TPU:0, one launch (start us, length us, event | category | flops | bytes accessed | tf_op | source)
XLA Modules:
  0.0 224.1 jit_solution(17769417152890954253)
XLA Ops:
  11.2 11.4 %psum.14 = f32[256]{0:T(256)S(1)} all-reduce(f32[256]{0:T(256)S(1)} %fusion.59), channel_id=1, replica_groups=mesh['sp'=8,'tp'=4] {'tp'}, use_global_device_ids=true, to_apply=%region_1.0 | all-reduce | flops 256 | bytes 2048 | tf_op jit(solution)/shard_map/psum | solution.py:107
  23.7 11.3 %all_gather.18 = bf16[256,1024]{1,0:T(8,128)(2,1)S(1)} all-gather(bf16[256,256]{1,0:T(8,128)(2,1)S(1)} %fusion.61), channel_id=1, replica_groups=mesh['sp'=8,'tp'=4] {'tp'}, dimensions={1}, use_global_device_ids=true | all-gather | bytes 655360 | tf_op jit(solution)/shard_map/all_gather | solution.py:18
  35.1 1.4 fusion.79
  37.6 5.7 %fusion.10 = f32[64,64,4,4,12]{1,4,3,2,0:T(8,128)} fusion(f32[64,64,4,15]{1,3,2,0:T(8,128)S(1)} %fusion.53, s32[4,12]{1,0:T(4,128)S(1)} %subtract_add_fusion.1), kind=kOutput, calls=%fused_computation.16 | convolution fusion | flops 141558480 | bytes 4128960 | tf_op jit(solution)/shard_map/hab,ria,qkb->rhqik/dot_general | solution.py:66
  43.3 2.1 slice_bitcast_fusion.2
  45.4 12.6 %all-gather.5.cloned.1.call-done = bf16[2,1024,256]{2,1,0:T(8,128)(2,1)} async-done(((bf16[2,128,256]{2,1,0:T(8,128)(2,1)}), bf16[2,1024,256]{2,1,0:T(8,128)(2,1)}) %all-gather.5.cloned.1.call-update) | async-done | bytes 1048592 | tf_op jit(solution)/shard_map/all_gather | solution.py:94
  58.0 2.1 slice_bitcast_fusion.4
  60.1 21.7 %all-gather.7.cloned.1.call-done = bf16[2,1024,256]{2,1,0:T(8,128)(2,1)} async-done(((bf16[2,128,256]{2,1,0:T(8,128)(2,1)}), bf16[2,1024,256]{2,1,0:T(8,128)(2,1)}) %all-gather.7.cloned.1.call-update) | async-done | bytes 1048592 | tf_op jit(solution)/shard_map/all_gather | solution.py:95
  81.8 2.1 slice_bitcast_fusion.3
  84.5 2.1 collective-permute-start
  86.6 1.3 collective-permute-start.1
  87.9 9.8 %copy.30 = f32[64,64,4,4,12]{0,1,3,4,2:T(8,128)} copy(f32[64,64,4,4,12]{1,4,3,2,0:T(8,128)} %fusion.10) | data formatting | bytes 6291456 | tf_op jit(solution)/shard_map/hab,ria,qkb->rhqik/dot_general | solution.py:66
  99.0 4.5 %fusion.80 = (f32[4,4,64]{2,0,1:T(4,128)S(1)}, f32[4,4,64,12,64]{2,4,0,3,1:T(8,128)S(1)}) fusion(f32[64,64,4,4,12]{0,1,3,4,2:T(8,128)} %copy.30, bf16[4,64,4,64,1]{3,2,1,0,4:T(4,128)(2,1)S(1)} %bitcast.99, bf16[12,64,4,64,1]{3,2,1,0,4:T(4,128)(2,1)S(1)} %bitcast.97, pred[4,64,12,64]{1,3,0,2:T(8,128)(4,1)S(1)} %broadcast_and_fusion), kind=kOutput, calls=%fused_computation.106 | convolution fusion | flops 103808000 | bytes 7016448 | tf_op jit(solution)/shard_map/rqhd,ikhd->rhqik/dot_general | solution.py:73
  107.4 2.1 fusion.36
  109.7 1.8 fusion.51
  111.4 24.0 %reduce-scatter.3.cloned.1.call-done = bf16[256,256]{0,1:T(8,128)(2,1)} async-done(((bf16[1024,256]{0,1:T(8,128)(2,1)}), bf16[256,256]{0,1:T(8,128)(2,1)}) %reduce-scatter.3.cloned.1.call-update) | async-done | bytes 131088 | tf_op jit(solution)/shard_map/reduce_scatter | solution.py:40
  136.4 9.1 %psum.15 = f32[256]{0:T(256)S(1)} all-reduce(f32[256]{0:T(256)S(1)} %fusion.62), channel_id=1, replica_groups=mesh['sp'=8,'tp'=4] {'tp'}, use_global_device_ids=true, to_apply=%region_6.7 | all-reduce | flops 256 | bytes 2048 | tf_op jit(solution)/shard_map/psum | solution.py:107
  146.6 12.1 %all_gather.23 = bf16[256,1024]{1,0:T(8,128)(2,1)S(1)} all-gather(bf16[256,256]{1,0:T(8,128)(2,1)S(1)} %fusion.67), channel_id=1, replica_groups=mesh['sp'=8,'tp'=4] {'tp'}, dimensions={1}, use_global_device_ids=true | all-gather | bytes 655360 | tf_op jit(solution)/shard_map/all_gather | solution.py:18
  158.7 2.0 fusion.24
  160.7 1.3 collective-permute-start.2
  163.3 5.7 %fusion.8 = f32[64,64,4,4,12]{1,4,3,2,0:T(8,128)} fusion(f32[64,64,4,15]{1,3,2,0:T(8,128)S(1)} %fusion.51, s32[4,12]{1,0:T(4,128)S(1)} %subtract_add_fusion.1), kind=kOutput, calls=%fused_computation.14 | convolution fusion | flops 141558480 | bytes 4128960 | tf_op jit(solution)/shard_map/hab,ria,qkb->rhqik/dot_general | solution.py:66
  168.9 9.8 %copy.38 = f32[64,64,4,4,12]{0,1,3,4,2:T(8,128)} copy(f32[64,64,4,4,12]{1,4,3,2,0:T(8,128)} %fusion.8) | data formatting | bytes 6291456 | tf_op jit(solution)/shard_map/hab,ria,qkb->rhqik/dot_general | solution.py:66
  180.7 4.5 %fusion.81 = (f32[4,4,64]{2,0,1:T(4,128)S(1)}, f32[4,4,64,12,64]{2,4,0,3,1:T(8,128)S(1)}) fusion(f32[64,64,4,4,12]{0,1,3,4,2:T(8,128)} %copy.38, bf16[4,64,4,64,1]{3,2,1,0,4:T(4,128)(2,1)S(1)} %bitcast.98, bf16[12,64,4,64,1]{3,2,1,0,4:T(4,128)(2,1)S(1)} %bitcast.96, pred[4,64,12,64]{1,3,0,2:T(8,128)(4,1)S(1)} %broadcast_and_fusion), kind=kOutput, calls=%fused_computation.107 | convolution fusion | flops 103808000 | bytes 7016448 | tf_op jit(solution)/shard_map/rqhd,ikhd->rhqik/dot_general | solution.py:73
  189.0 28.2 %reduce-scatter.5.cloned.1.call-done = bf16[256,256]{0,1:T(8,128)(2,1)} async-done(((bf16[1024,256]{0,1:T(8,128)(2,1)}), bf16[256,256]{0,1:T(8,128)(2,1)}) %reduce-scatter.5.cloned.1.call-update) | async-done | bytes 131088 | tf_op jit(solution)/shard_map/reduce_scatter | solution.py:40
  (63 shorter events, 21.7 us)
Async XLA Ops:
  6.5 36.8 %all-gather.9.cloned.1.call-start = ((), (), s32[]{:S(2)}) async-start(), calls=%async_computation.4 | async-start | bytes 1179648 | tf_op jit(solution)/shard_map/all_gather | solution.py:96
  7.3 50.8 %all-gather.5.cloned.1.call-start = ((), (), s32[]{:S(2)}) async-start(), calls=%async_computation.2 | async-start | bytes 1179648 | tf_op jit(solution)/shard_map/all_gather | solution.py:94
  8.0 73.8 %all-gather.7.cloned.1.call-start = ((), (), s32[]{:S(2)}) async-start(), calls=%async_computation.3 | async-start | bytes 1179648 | tf_op jit(solution)/shard_map/all_gather | solution.py:95
  8.7 98.7 %all-gather.11.cloned.1.call-start = ((), (), s32[]{:S(2)}) async-start(), calls=%async_computation.5 | async-start | bytes 1179648 | tf_op jit(solution)/shard_map/all_gather | solution.py:97
  9.3 126.1 %reduce-scatter.3.cloned.1.call-start = ((), (), s32[]{:S(2)}) async-start(), calls=%async_computation.6 | async-start | bytes 655360 | tf_op jit(solution)/shard_map/reduce_scatter | solution.py:40
  84.5 13.7 %collective-permute-start = (bf16[4,64,512]{2,1,0:T(8,128)(2,1)S(1)}, bf16[4,64,512]{2,1,0:T(8,128)(2,1)S(1)}, u32[]{:S(2)}, u32[]{:S(2)}) collective-permute-start(bf16[4,64,512]{2,1,0:T(8,128)(2,1)S(1)} %bitcast.100), channel_id=1, source_target_pairs={{0,4},{4,8},{8,12},{12,16},{16,20},{20,24},{24,28},{1,5},{5,9},{9,... | collective-permute-start | bytes 786440 | tf_op jit(solution)/shard_map/ppermute | solution.py:29
  86.6 11.5 %collective-permute-start.1 = (bf16[4,64,512]{2,1,0:T(8,128)(2,1)S(1)}, bf16[4,64,512]{2,1,0:T(8,128)(2,1)S(1)}, u32[]{:S(2)}, u32[]{:S(2)}) collective-permute-start(bf16[4,64,512]{2,1,0:T(8,128)(2,1)S(1)} %bitcast.101), channel_id=1, source_target_pairs={{4,0},{8,4},{12,8},{16,12},{20,16},{24,20},{28,24},{5,1},{9,5},{13... | collective-permute-start | bytes 786440 | tf_op jit(solution)/shard_map/ppermute | solution.py:32
  109.6 107.6 %reduce-scatter.5.cloned.1.call-start = ((), (), s32[]{:S(2)}) async-start(), calls=%async_computation.7 | async-start | bytes 655360 | tf_op jit(solution)/shard_map/reduce_scatter | solution.py:40
  160.7 18.2 %collective-permute-start.2 = (bf16[4,64,512]{2,1,0:T(8,128)(2,1)S(1)}, bf16[4,64,512]{2,1,0:T(8,128)(2,1)S(1)}, u32[]{:S(2)}, u32[]{:S(2)}) collective-permute-start(bf16[4,64,512]{2,1,0:T(8,128)(2,1)S(1)} %bitcast.103), channel_id=1, source_target_pairs={{0,4},{4,8},{8,12},{12,16},{16,20},{20,24},{24,28},{1,5},{5,9},{9,... | collective-permute-start | bytes 786440 | tf_op jit(solution)/shard_map/ppermute | solution.py:29
  162.0 16.9 %collective-permute-start.3 = (bf16[4,64,512]{2,1,0:T(8,128)(2,1)S(1)}, bf16[4,64,512]{2,1,0:T(8,128)(2,1)}, u32[]{:S(2)}, u32[]{:S(2)}) collective-permute-start(bf16[4,64,512]{2,1,0:T(8,128)(2,1)S(1)} %bitcast.104), channel_id=1, source_target_pairs={{4,0},{8,4},{12,8},{16,12},{20,16},{24,20},{28,24},{5,1},{9,5},{13... | collective-permute-start | bytes 786440 | tf_op jit(solution)/shard_map/ppermute | solution.py:32
  186.3 1.6 copy-start
Sparse Core Ops, SparseCore 0:
  8.9 25.2 all-gather.8
  35.8 22.1 all-gather.4
  59.6 22.1 all-gather.6
  83.2 24.1 all-gather.10
  110.1 25.2 reduce-scatter.2
  189.1 28.0 reduce-scatter.4
where the time goes:
time: 225 us; the launch traced here: 224 us
  waiting for transfers between devices  90.4 us (40%)
  blocking collectives  43.9 us (20%)
  matrix products  31.3 us (14%)
  local copies, waits for them, and re-layouts  29.7 us (13%)
  between operations  13.8 us (6%)
  other arithmetic  8.54 us (4%)
  starting transfers between devices  6.23 us (3%)
    reduce_scatter x2, waiting for transfers between devices, own_rows(): lax.psum_scatter(sent, axis, scatter_dimension=0, tiled=True)  52.2 us
    all_gather x2, blocking collectives, folded(): lax.all_gather(part, axis, axis=dim, tiled=True)  23.4 us
    all_gather x1, waiting for transfers between devices, body(): lax.all_gather(key_weight, 'sp', axis=1, tiled=True)  21.7 us
    psum x2, blocking collectives, body(): squares = lax.psum(jnp.sum(floats * floats, axis=1), 'tp')  20.5 us
    dot_general x2, local copies, waits for them, and re-layouts, attend(): jnp.einsum('hab,ria,qkb->rhqik', table, row_onehot, col_onehot, precision...  19.5 us
    dot_general x4, matrix products, attend(): jnp.einsum('hab,ria,qkb->rhqik', table, row_onehot, col_onehot, precision...  14.2 us
    all_gather x1, waiting for transfers between devices, body(): lax.all_gather(query_weight, 'sp', axis=1, tiled=True)  12.6 us
    dot_general x2, matrix products, attend(): jnp.einsum('rqhd,ikhd->rhqik', grid_query, keys, preferred_element_type=j...  9.03 us
  transfers between devices with their start and end apart: 10, of which 5 were waited for; matrix products, arithmetic and copies ran while one was open for 24% of the time, Pallas kernels for 0%

commit v1 on v0

--- a/solution.py
+++ b/solution.py
@@ -1,7 +1,13 @@
+import functools
+
 import jax
 import jax.numpy as jnp
 from jax import lax
+from jax.experimental import pallas as pl
+from jax.experimental.pallas import tpu as pltpu
 from jax.sharding import PartitionSpec as P
+
+MESH = pl.DeviceIdType.MESH
 
 HEAD_DIM = 64
 WIN_H = 8
@@ -14,9 +20,114 @@
 norm_eps = 1e-06
 
 
-def folded(value, axis, dim, update, carry):
-    whole = jax.tree.map(lambda part: lax.all_gather(part, axis, axis=dim, tiled=True), value)
-    return update(carry, whole, jnp.int32(0))
+def greet(me, n):
+    barrier = pltpu.get_barrier_semaphore()
+    for k in range(1, n):
+        pl.semaphore_signal(
+            barrier, inc=1, device_id={"tp": lax.rem(me + k, n)}, device_id_type=MESH
+        )
+    pl.semaphore_wait(barrier, n - 1)
+
+
+def norm_kernel(n, x_ref, gain_ref, out_ref, held, gains, send, recv, gain_send, gain_recv):
+    me = lax.axis_index("tp")
+    width = x_ref.shape[1]
+    greet(me, n)
+    copies = []
+    for k in range(1, n):
+        peer = {"tp": lax.rem(me + k, n)}
+        copies.append((
+            pltpu.make_async_remote_copy(
+                src_ref=x_ref, dst_ref=held.at[k - 1], send_sem=send.at[k - 1],
+                recv_sem=recv.at[k - 1], device_id=peer, device_id_type=MESH,
+            ),
+            pltpu.make_async_remote_copy(
+                src_ref=gain_ref, dst_ref=gains.at[k - 1], send_sem=gain_send.at[k - 1],
+                recv_sem=gain_recv.at[k - 1], device_id=peer, device_id_type=MESH,
+            ),
+        ))
+    for big, small in copies:
+        big.start()
+        small.start()
+    own = x_ref[...].astype(jnp.float32)
+    squares = jnp.sum(own * own, axis=1, keepdims=True)
+    for k, (big, small) in enumerate(copies):
+        big.wait()
+        small.wait()
+        part = held[k].astype(jnp.float32)
+        squares = squares + jnp.sum(part * part, axis=1, keepdims=True)
+    factor = lax.rsqrt(squares / (n * width) + norm_eps)
+    for k in range(n):
+        block = x_ref[...] if k == 0 else held[k - 1]
+        gain = gain_ref[...] if k == 0 else gains[k - 1]
+        scaled = block.astype(jnp.float32) * factor * gain[0:1].astype(jnp.float32)
+        source = lax.rem(me - k + n, n)
+        if len(out_ref.shape) == 2:
+            columns = pl.ds(pl.multiple_of(source * width, width), width)
+            out_ref[:, columns] = scaled.astype(jnp.bfloat16)
+        else:
+            out_ref[source] = scaled.astype(jnp.bfloat16)
+
+
+def gathered_norm(current, gain, n, ident):
+    count, width = current.shape
+    wide = jnp.broadcast_to(gain[None, :], (16, width))
+    flat = width % 128 == 0
+    shape = (count, n * width) if flat else (n, count, width)
+    vmem = pl.BlockSpec(memory_space=pltpu.VMEM)
+    out = pl.pallas_call(
+        functools.partial(norm_kernel, n),
+        out_shape=jax.ShapeDtypeStruct(shape, jnp.bfloat16),
+        in_specs=[vmem] * 2,
+        out_specs=vmem,
+        scratch_shapes=[
+            pltpu.VMEM((n - 1, count, width), jnp.bfloat16),
+            pltpu.VMEM((n - 1, 16, width), jnp.bfloat16),
+        ] + [pltpu.SemaphoreType.DMA((n - 1,))] * 4,
+        compiler_params=pltpu.CompilerParams(collective_id=ident, has_side_effects=True),
+    )(current, wide)
+    return out if flat else out.transpose(1, 0, 2).reshape(count, n * width)
+
+
+def sum_kernel(n, x_ref, w_ref, out_ref, parts, held, send, recv):
+    me = lax.axis_index("tp")
+    width = out_ref.shape[1]
+    for j in range(n):
+        parts[j] = jnp.dot(
+            x_ref[...], w_ref[:, j * width:(j + 1) * width], preferred_element_type=jnp.float32
+        ).astype(jnp.bfloat16)
+    greet(me, n)
+    copies = []
+    for k in range(1, n):
+        peer = lax.rem(me + k, n)
+        copies.append(pltpu.make_async_remote_copy(
+            src_ref=parts.at[peer], dst_ref=held.at[k - 1], send_sem=send.at[k - 1],
+            recv_sem=recv.at[k - 1], device_id={"tp": peer}, device_id_type=MESH,
+        ))
+    for copy in copies:
+        copy.start()
+    total = parts[me].astype(jnp.float32)
+    for k, copy in enumerate(copies):
+        copy.wait()
+        total = total + held[k].astype(jnp.float32)
+    out_ref[...] = total.astype(jnp.bfloat16)
+
+
+def projected_sum(attended, weight, n, ident):
+    count = attended.shape[0]
+    width = weight.shape[1] // n
+    vmem = pl.BlockSpec(memory_space=pltpu.VMEM)
+    return pl.pallas_call(
+        functools.partial(sum_kernel, n),
+        out_shape=jax.ShapeDtypeStruct((count, width), jnp.bfloat16),
+        in_specs=[vmem] * 2,
+        out_specs=vmem,
+        scratch_shapes=[
+            pltpu.VMEM((n, count, width), jnp.bfloat16),
+            pltpu.VMEM((n - 1, count, width), jnp.bfloat16),
+        ] + [pltpu.SemaphoreType.DMA((n - 1,))] * 2,
+        compiler_params=pltpu.CompilerParams(collective_id=ident, has_side_effects=True),
+    )(attended, weight)
 
 
 def extended(block, sides, width, periodic):
@@ -32,12 +143,6 @@
         high = lax.ppermute(lax.slice_in_dim(block, 0, width, axis=dim), axis, backward)
         block = jnp.concatenate([low, block, high], axis=dim)
     return block
-
-
-def own_rows(portion, rows, axis):
-    count = rows * lax.axis_size(axis)
-    sent = portion(jnp.int32(0), count).astype(jnp.bfloat16)
-    return lax.psum_scatter(sent, axis, scatter_dimension=0, tiled=True).astype(jnp.float32)
 
 
 def attend(query, padded, table, base, total_rows):
@@ -85,52 +190,32 @@
 def body(tokens, norm_gain, query_weight, key_weight, value_weight, output_weight, offset_bias):
     layers = query_weight.shape[0]
     local_width = query_weight.shape[2]
-    feature_rows = tokens.shape[1]
-    token_count = tokens.shape[0]
+    n = lax.axis_size("tp")
     half = WIN_H // 2
     base = lax.axis_index("sp") * ROWS_DEV
     total_rows = ROWS_DEV * lax.axis_size("sp")
-    every = (
-        lax.all_gather(query_weight, "sp", axis=1, tiled=True),
-        lax.all_gather(key_weight, "sp", axis=1, tiled=True),
-        lax.all_gather(value_weight, "sp", axis=1, tiled=True),
-        lax.all_gather(output_weight, "sp", axis=2, tiled=True),
-    )
     current = tokens
+    every = []
     for layer in range(layers):
-        query_full = every[0][layer]
-        key_full = every[1][layer]
-        value_full = every[2][layer]
-        output_full = every[3][layer]
-        stacked = jnp.concatenate([query_full, key_full, value_full], axis=1)
-        floats = current.astype(jnp.float32)
-        squares = lax.psum(jnp.sum(floats * floats, axis=1), "tp")
-        factor = lax.rsqrt(squares / D + norm_eps)
-        normed = (floats * factor[:, None] * norm_gain[layer].astype(jnp.float32)).astype(
+        own = jnp.concatenate(
+            [query_weight[layer], key_weight[layer], value_weight[layer]], axis=1
+        )
+        every.append((
+            lax.all_gather(own, "sp", axis=0, tiled=True),
+            lax.all_gather(output_weight[layer], "sp", axis=1, tiled=True),
+        ))
+    for layer in range(layers):
+        stacked, output_full = every[layer]
+        normed = gathered_norm(current, norm_gain[layer], n, 2 * layer)
+        table = offset_bias[layer].astype(jnp.float32)
+        projected = jnp.dot(normed, stacked, preferred_element_type=jnp.float32).astype(
             jnp.bfloat16
         )
-        table = offset_bias[layer].astype(jnp.float32)
-
-        def project(carry, piece, start):
-            weight_rows = lax.dynamic_slice_in_dim(stacked, start, piece.shape[1], 0)
-            return carry + jnp.dot(piece, weight_rows, preferred_element_type=jnp.float32)
-
-        projected = folded(
-            normed, "tp", 1, project, jnp.zeros((token_count, 3 * local_width), jnp.float32)
-        ).astype(jnp.bfloat16)
         query = projected[:, :local_width]
         pair = projected[:, local_width:].reshape(ROWS_DEV, COLS, 2 * local_width)
         padded = extended(pair, (("sp", 0),), half, False)
         attended = attend(query, padded, table, base, total_rows)
-
-        def project_out(start, count):
-            weight_cols = lax.dynamic_slice_in_dim(output_full, start, count, 1)
-            return lax.dot_general(
-                weight_cols, attended, (((0,), (1,)), ((), ())), preferred_element_type=jnp.float32
-            )
-
-        summed = own_rows(project_out, feature_rows, "tp")
-        current = summed.T.astype(jnp.bfloat16)
+        current = projected_sum(attended, output_full, n, 2 * layer + 1)
     return current
 
 

time: 225 us -> 179 us (0.80)
  waiting for transfers between devices: 90.4 us -> 1.5 us
  Pallas kernels: 0 us -> 44.1 us
  local copies, waits for them, and re-layouts: 29.7 us -> 35 us
  blocking collectives: 43.9 us -> 40.3 us
  other arithmetic: 8.54 us -> 6.07 us
    reduce_scatter x2 -> x0, waiting for transfers between devices: 52.2 us -> none  [own_rows(): lax.psum_scatter(sent, axis, scatter_dimension=0, tiled=True)]
    pallas_call x0 -> x4, Pallas kernels: none -> 44.1 us  [the longest x2 23.5 us: gathered_norm(): pl.pallas_call(functools.partial(norm_kernel, n), out_shape=jax.ShapeDtyp...]
    all_gather x4 -> x2, waiting for transfers between devices: 35.6 us -> 0.04 us  [body(): lax.all_gather(own, 'sp', axis=0, tiled=True)]
    psum x2 -> x0, blocking collectives: 20.5 us -> none  [body(): squares = lax.psum(jnp.sum(floats * floats, axis=1), 'tp')]
    all_gather x2, blocking collectives: 23.4 us -> 40.3 us  [body(): lax.all_gather(output_weight[layer], 'sp', axis=1, tiled=True)]
    squeeze x3 -> x2, local copies, waits for them, and re-layouts: 6.2 us -> 1.84 us  [the longest x1 0.96 us: body(): value_weight[layer]]
    unnamed x6 -> x2, waiting for transfers between devices: 2.64 us -> 0.03 us
    dot_general x4 -> x2, matrix products: 5.77 us -> 4.29 us  [body(): jnp.dot(normed, stacked, preferred_element_type=jnp.float32)]
  transfers between devices with their start and end apart: 10 -> 6, of which waited for: 5 -> 1; matrix products, arithmetic and copies ran while one was open for 24% -> 31% of each run, Pallas kernels for 0% -> 19%
where the time goes in v1:
time: 179 us; the launch traced here: 177 us
  Pallas kernels  44.1 us (25%)
  blocking collectives  40.3 us (23%)
  local copies, waits for them, and re-layouts  35 us (20%)
  matrix products  29.1 us (16%)
  between operations  13.7 us (8%)
  starting transfers between devices  7.47 us (4%)
  other arithmetic  6.07 us (3%)
    all_gather x2, blocking collectives, body(): lax.all_gather(output_weight[layer], 'sp', axis=1, tiled=True)  40.3 us
    pallas_call x2, Pallas kernels, gathered_norm(): pl.pallas_call(functools.partial(norm_kernel, n), out_shape=jax.ShapeDtyp...  23.5 us
    pallas_call x2, Pallas kernels, projected_sum(): pl.pallas_call(functools.partial(sum_kernel, n), out_shape=jax.ShapeDtype...  20.7 us
    dot_general x2, local copies, waits for them, and re-layouts, attend(): jnp.einsum('hab,ria,qkb->rhqik', table, row_onehot, col_onehot, precision...  19.6 us
    dot_general x4, matrix products, attend(): jnp.einsum('hab,ria,qkb->rhqik', table, row_onehot, col_onehot, precision...  13.4 us
    dot_general x2, matrix products, attend(): jnp.einsum('rqhd,ikhd->rhqik', grid_query, keys, preferred_element_type=j...  9.03 us
    ppermute x2, starting transfers between devices, extended(): lax.ppermute(lax.slice_in_dim(block, block.shape[dim] - width, None, axis...  4.67 us
    dot_general x2, matrix products, body(): jnp.dot(normed, stacked, preferred_element_type=jnp.float32)  4.29 us
  transfers between devices with their start and end apart: 6, of which 1 were waited for; matrix products, arithmetic and copies ran while one was open for 31% of the time, Pallas kernels for 19%

profile of v1, /device:TPU:0, one launch (start us, length us, event | category | flops | bytes accessed | tf_op | source)
XLA Modules:
  0.0 177.4 jit_solution(677380286291122890)
XLA Ops:
  12.8 5.7 %fusion.10 = f32[64,64,4,4,12]{1,4,3,2,0:T(8,128)} fusion(f32[64,64,4,15]{1,3,2,0:T(8,128)S(1)} %fusion.33, s32[4,12]{1,0:T(4,128)S(1)} %subtract_add_fusion.1), kind=kOutput, calls=%fused_computation.16 | convolution fusion | flops 141558480 | bytes 4128960 | tf_op jit(solution)/shard_map/hab,ria,qkb->rhqik/dot_general | solution.py:171
  18.4 9.8 %copy.32 = f32[64,64,4,4,12]{0,1,3,4,2:T(8,128)} copy(f32[64,64,4,4,12]{1,4,3,2,0:T(8,128)} %fusion.10) | data formatting | bytes 6291456 | tf_op jit(solution)/shard_map/hab,ria,qkb->rhqik/dot_general | solution.py:171
  28.9 18.3 %all-gather = bf16[1,256,1024]{2,1,0:T(8,128)(2,1)} all-gather(bf16[1,256,128]{2,1,0:T(8,128)(2,1)S(1)} %get-tuple-element.12), channel_id=2, replica_groups=mesh['sp'=8,'tp'=4] {'sp'}, dimensions={2}, use_global_device_ids=true | all-gather | bytes 589824 | tf_op jit(solution)/shard_map/all_gather | solution.py:205
  47.8 11.8 %shard_map.73 = bf16[256,1024]{1,0:T(8,128)(2,1)} custom-call(bf16[256,256]{1,0:T(8,128)(2,1)} %x_ref.1, bf16[16,256]{1,0:T(8,128)(2,1)} %broadcast_in_dim.21.gain_ref), custom_call_target="tpu_custom_call" | custom-call | tf_op jit(solution)/shard_map/pallas_call | solution.py:78
  59.9 2.1 %convolution_convert_fusion.1 = bf16[256,768]{1,0:T(8,128)(2,1)S(1)} fusion(bf16[256,1024]{1,0:T(8,128)(2,1)} %shard_map.73, bf16[1024,768]{1,0:T(8,128)(2,1)} %all-gather.5.cloned.1.call-done), kind=kOutput, calls=%fused_computation.19 | convolution fusion | flops 402849792 | bytes 2490368 | tf_op jit(solution)/shard_map/dot_general | solution.py:211
  62.1 1.8 %collective-permute-start = (bf16[4,64,512]{2,1,0:T(8,128)(2,1)S(1)}, bf16[4,64,512]{2,1,0:T(8,128)(2,1)S(1)}, u32[]{:S(2)}, u32[]{:S(2)}) collective-permute-start(bf16[4,64,512]{2,1,0:T(8,128)(2,1)S(1)} %bitcast.92), channel_id=1, source_target_pairs={{0,4},{4,8},{8,12},{12,16},{16,20},{20,24},{24,28},{1,5},{5,9},{9,... | collective-permute-start | bytes 786440 | tf_op jit(solution)/shard_map/ppermute | solution.py:140
  63.9 1.5 collective-permute-start.1
  66.6 1.4 collective-permute-done.1
  70.1 1.8 %reshape.195 = bf16[12,64,4,64]{3,2,1,0:T(4,128)(2,1)S(1)} reshape(bf16[12,64,256]{2,1,0:T(8,128)(2,1)} %get-tuple-element.10) | data formatting | bytes 786432 | tf_op jit(solution)/shard_map/reshape | solution.py:175
  71.9 2.6 %reshape.194 = bf16[12,64,4,64]{3,2,1,0:T(4,128)(2,1)} reshape(bf16[12,64,256]{2,1,0:T(8,128)(2,1)} %get-tuple-element.9) | data formatting | bytes 786432 | tf_op jit(solution)/shard_map/reshape | solution.py:176
  74.5 4.5 %fusion.52 = (f32[4,4,64]{2,0,1:T(4,128)S(1)}, f32[4,4,64,12,64]{2,4,0,3,1:T(8,128)S(1)}) fusion(f32[64,64,4,4,12]{0,1,3,4,2:T(8,128)} %copy.32, bf16[4,64,4,64,1]{3,2,1,0,4:T(4,128)(2,1)S(1)} %bitcast.88, bf16[12,64,4,64,1]{3,2,1,0,4:T(4,128)(2,1)S(1)} %bitcast.84, pred[4,64,12,64]{1,3,0,2:T(8,128)(4,1)S(1)} %broadcast_and_fusion), kind=kOutput, calls=%fused_computation.76 | convolution fusion | flops 103808000 | bytes 7016448 | tf_op jit(solution)/shard_map/rqhd,ikhd->rhqik/dot_general | solution.py:178
  80.2 1.2 fusion.24
  82.4 9.7 %shard_map.74.x_ref = bf16[256,256]{1,0:T(8,128)(2,1)} custom-call(bf16[256,256]{1,0:T(8,128)(2,1)} %reshape.197.x_ref, bf16[256,1024]{1,0:T(8,128)(2,1)} %bitcast.85), custom_call_target="tpu_custom_call" | custom-call | tf_op jit(solution)/shard_map/pallas_call | solution.py:120
  92.7 11.6 %shard_map.75 = bf16[256,1024]{1,0:T(8,128)(2,1)} custom-call(bf16[256,256]{1,0:T(8,128)(2,1)} %shard_map.74.x_ref, bf16[16,256]{1,0:T(8,128)(2,1)} %broadcast_in_dim.29.gain_ref), custom_call_target="tpu_custom_call" | custom-call | tf_op jit(solution)/shard_map/pallas_call | solution.py:78
  104.3 2.1 %convolution_convert_fusion = bf16[256,768]{1,0:T(8,128)(2,1)S(1)} fusion(bf16[256,1024]{1,0:T(8,128)(2,1)} %shard_map.75, bf16[1024,768]{1,0:T(8,128)(2,1)} %all-gather.7.cloned.1.call-done), kind=kOutput, calls=%fused_computation.18 | convolution fusion | flops 402849792 | bytes 2490368 | tf_op jit(solution)/shard_map/dot_general | solution.py:211
  106.5 2.9 %collective-permute-start.2 = (bf16[4,64,512]{2,1,0:T(8,128)(2,1)S(1)}, bf16[4,64,512]{2,1,0:T(8,128)(2,1)S(1)}, u32[]{:S(2)}, u32[]{:S(2)}) collective-permute-start(bf16[4,64,512]{2,1,0:T(8,128)(2,1)S(1)} %bitcast.89), channel_id=1, source_target_pairs={{0,4},{4,8},{8,12},{12,16},{16,20},{20,24},{24,28},{1,5},{5,9},{9,... | collective-permute-start | bytes 786440 | tf_op jit(solution)/shard_map/ppermute | solution.py:140
  109.4 1.3 collective-permute-start.3
  110.7 5.7 %fusion.8 = f32[64,64,4,4,12]{1,4,3,2,0:T(8,128)} fusion(f32[64,64,4,15]{1,3,2,0:T(8,128)S(1)} %fusion.31, s32[4,12]{1,0:T(4,128)S(1)} %subtract_add_fusion.1), kind=kOutput, calls=%fused_computation.14 | convolution fusion | flops 141558480 | bytes 4128960 | tf_op jit(solution)/shard_map/hab,ria,qkb->rhqik/dot_general | solution.py:171
  116.4 9.8 %copy.40 = f32[64,64,4,4,12]{0,1,3,4,2:T(8,128)} copy(f32[64,64,4,4,12]{1,4,3,2,0:T(8,128)} %fusion.8) | data formatting | bytes 6291456 | tf_op jit(solution)/shard_map/hab,ria,qkb->rhqik/dot_general | solution.py:171
  126.1 22.0 %all-gather.1 = bf16[1,256,1024]{2,1,0:T(8,128)(2,1)} all-gather(bf16[1,256,128]{2,1,0:T(8,128)(2,1)S(1)} %copy-done.1), channel_id=3, replica_groups=mesh['sp'=8,'tp'=4] {'sp'}, dimensions={2}, use_global_device_ids=true | all-gather | bytes 589824 | tf_op jit(solution)/shard_map/all_gather | solution.py:205
  150.1 4.5 %fusion.53 = (f32[4,4,64]{2,0,1:T(4,128)S(1)}, f32[4,4,64,12,64]{2,4,0,3,1:T(8,128)S(1)}) fusion(f32[64,64,4,4,12]{0,1,3,4,2:T(8,128)} %copy.40, bf16[4,64,4,64,1]{3,2,1,0,4:T(4,128)(2,1)S(1)} %bitcast.87, bf16[12,64,4,64,1]{3,2,1,0,4:T(4,128)(2,1)S(1)} %bitcast.83, pred[4,64,12,64]{1,3,0,2:T(8,128)(4,1)S(1)} %broadcast_and_fusion), kind=kOutput, calls=%fused_computation.77 | convolution fusion | flops 103808000 | bytes 7016448 | tf_op jit(solution)/shard_map/rqhd,ikhd->rhqik/dot_general | solution.py:178
  155.7 1.2 fusion.27
  157.9 11.0 %shard_map.76 = bf16[256,256]{1,0:T(8,128)(2,1)} custom-call(bf16[256,256]{1,0:T(8,128)(2,1)} %reshape.202.x_ref, bf16[256,1024]{1,0:T(8,128)(2,1)} %bitcast.86), custom_call_target="tpu_custom_call" | custom-call | tf_op jit(solution)/shard_map/pallas_call | solution.py:120
  168.9 1.6 copy.125
  (54 shorter events, 17.8 us)
Async XLA Ops:
  6.5 53.4 %all-gather.5.cloned.1.call-start = ((), (), s32[]{:S(2)}) async-start(), calls=%async_computation | async-start | bytes 1769472 | tf_op jit(solution)/shard_map/all_gather | solution.py:204
  9.1 95.2 %all-gather.7.cloned.1.call-start = ((), (), s32[]{:S(2)}) async-start(), calls=%async_computation.1 | async-start | bytes 1769472 | tf_op jit(solution)/shard_map/all_gather | solution.py:204
  18.4 9.8 %copy-start.2 = (bf16[2,256,128]{2,1,0:T(8,128)(2,1)S(1)}, bf16[2,256,128]{2,1,0:T(8,128)(2,1)}, u32[]{:S(2)}) copy-start(bf16[2,256,128]{2,1,0:T(8,128)(2,1)} %param.12) | copy-start | bytes 393220
  62.1 4.5 %collective-permute-start = (bf16[4,64,512]{2,1,0:T(8,128)(2,1)S(1)}, bf16[4,64,512]{2,1,0:T(8,128)(2,1)S(1)}, u32[]{:S(2)}, u32[]{:S(2)}) collective-permute-start(bf16[4,64,512]{2,1,0:T(8,128)(2,1)S(1)} %bitcast.92), channel_id=1, source_target_pairs={{0,4},{4,8},{8,12},{12,16},{16,20},{20,24},{24,28},{1,5},{5,9},{9,... | collective-permute-start | bytes 786440 | tf_op jit(solution)/shard_map/ppermute | solution.py:140
  63.9 4.1 %collective-permute-start.1 = (bf16[4,64,512]{2,1,0:T(8,128)(2,1)S(1)}, bf16[4,64,512]{2,1,0:T(8,128)(2,1)}, u32[]{:S(2)}, u32[]{:S(2)}) collective-permute-start(bf16[4,64,512]{2,1,0:T(8,128)(2,1)S(1)} %bitcast.93), channel_id=1, source_target_pairs={{4,0},{8,4},{12,8},{16,12},{20,16},{24,20},{28,24},{5,1},{9,5},{13... | collective-permute-start | bytes 786440 | tf_op jit(solution)/shard_map/ppermute | solution.py:143
  79.0 1.1 copy-start
  106.5 41.8 %collective-permute-start.2 = (bf16[4,64,512]{2,1,0:T(8,128)(2,1)S(1)}, bf16[4,64,512]{2,1,0:T(8,128)(2,1)S(1)}, u32[]{:S(2)}, u32[]{:S(2)}) collective-permute-start(bf16[4,64,512]{2,1,0:T(8,128)(2,1)S(1)} %bitcast.89), channel_id=1, source_target_pairs={{0,4},{4,8},{8,12},{12,16},{16,20},{20,24},{24,28},{1,5},{5,9},{9,... | collective-permute-start | bytes 786440 | tf_op jit(solution)/shard_map/ppermute | solution.py:140
  109.4 38.9 %collective-permute-start.3 = (bf16[4,64,512]{2,1,0:T(8,128)(2,1)S(1)}, bf16[4,64,512]{2,1,0:T(8,128)(2,1)}, u32[]{:S(2)}, u32[]{:S(2)}) collective-permute-start(bf16[4,64,512]{2,1,0:T(8,128)(2,1)S(1)} %bitcast.90), channel_id=1, source_target_pairs={{4,0},{8,4},{12,8},{16,12},{20,16},{24,20},{28,24},{5,1},{9,5},{13... | collective-permute-start | bytes 786440 | tf_op jit(solution)/shard_map/ppermute | solution.py:143
  116.4 9.8 %copy-start.1 = (bf16[1,256,128]{2,1,0:T(8,128)(2,1)S(1)}, bf16[1,256,128]{2,1,0:T(8,128)(2,1)}, u32[]{:S(2)}) copy-start(bf16[1,256,128]{2,1,0:T(8,128)(2,1)} %get-tuple-element.11) | copy-start | bytes 196612
Sparse Core Ops, SparseCore 0:
  9.2 28.0 all-gather.4
  38.9 24.9 all-gather.6
